TPU v7x, 32 devices: a whole 2x2x4 slice. The times are simulated.
32 devices in a mesh: fs: 4 (over y, x), tp: 8 (over z, core).
Axes of the slice: x: 2, y: 2, z: 4, core: 2. Of those that a mesh axis runs over, the one named last changes fastest.
Arguments:
- tokens: bfloat16 [4096, 2048], P(('fs', 'tp')), may hold values from -6 to 6
- norm_gain: float32 [2048], P('fs'), may hold values from 0.1 to 1.9
- gate_master: float32 [2048, 8192], P('fs', 'tp'), may hold values from -0.125 to 0.125
- up_master: float32 [2048, 8192], P('fs', 'tp'), may hold values from -0.125 to 0.125
- down_master: float32 [2048, 8192], P('fs', 'tp'), may hold values from -0.09375 to 0.09375
Outputs:
- mixed: bfloat16 [4096, 2048], P(('fs', 'tp'))
- gate_ready: bfloat16 [2048, 8192], P(None, 'tp')
- up_ready: bfloat16 [2048, 8192], P(None, 'tp')
- down_ready: bfloat16 [2048, 8192], P(None, 'tp')
All inputs are finite; a program needn't handle non-finite values.
Results may differ from a plain program's by a relative error of at most 0.0095.
Values may be sent and summed in bfloat16 or wider, within the bound.
A program may use at most 64 MiB of HBM per device.

v0:
```python
import jax
import jax.numpy as jnp
from jax import lax
from jax.sharding import PartitionSpec as P


def expand_rows(rows, gate_ready, up_ready):
    rows_wide = rows.astype(jnp.float32)
    row_scale = lax.rsqrt(jnp.mean(rows_wide * rows_wide, axis=1, keepdims=True) + 1e-06)
    gate_proj = row_scale * jnp.dot(rows, gate_ready, preferred_element_type=jnp.float32)
    up_proj = row_scale * jnp.dot(rows, up_ready, preferred_element_type=jnp.float32)
    return (jax.nn.silu(gate_proj) * up_proj).astype(jnp.bfloat16)


def body(tokens, norm_gain, gate_master, up_master, down_master):
    gate_local = (norm_gain[:, None] * gate_master).astype(jnp.bfloat16)
    up_local = (norm_gain[:, None] * up_master).astype(jnp.bfloat16)
    down_local = down_master.astype(jnp.bfloat16)
    gate_ready, up_ready, down_ready = (
        lax.all_gather(gate_local, "fs", axis=0, tiled=True),
        lax.all_gather(up_local, "fs", axis=0, tiled=True),
        lax.all_gather(down_local, "fs", axis=0, tiled=True),
    )
    hidden = expand_rows(lax.all_gather(tokens, "tp", axis=0, tiled=True), gate_ready, up_ready)
    partial_value = lax.dot_general(
        hidden, down_ready, (((1,), (1,)), ((), ())), preferred_element_type=jnp.float32
    )
    summed = lax.psum_scatter(
        partial_value.astype(jnp.bfloat16), "tp", scatter_dimension=0, tiled=True
    ).astype(jnp.float32)
    mixed = (tokens.astype(jnp.float32) + 0.5 * summed).astype(jnp.bfloat16)
    return (mixed, gate_ready, up_ready, down_ready)


def solution(mesh):
    in_specs = (P(("fs", "tp"), None), P("fs"), P("fs", "tp"), P("fs", "tp"), P("fs", "tp"))
    out_specs = (P(("fs", "tp"), None), P(None, "tp"), P(None, "tp"), P(None, "tp"))
    return jax.shard_map(body, mesh=mesh, in_specs=in_specs, out_specs=out_specs, check_vma=False)
```

profile of v0, /device:TPU:0, one launch (start us, length us, event | category | flops | bytes accessed | tf_op | source)
XLA Modules:
  0.0 308.0 jit_solution(15317283137580708099)
XLA Ops:
  7.2 0.0 copy-start.3
  7.2 0.0 all-gather.5.cloned.1.call-start
  7.2 0.7 all-gather.5.cloned.1.call-update
  7.9 0.0 all-gather.7.cloned.1.call-start
  8.0 3.8 %multiply_convert_fusion = (bf16[512,1024]{1,0:T(8,128)(2,1)}, bf16[512,1024]{1,0:T(8,128)(2,1)}) fusion(f32[512,1024]{1,0:T(8,128)} %param.8, f32[512]{0:T(512)} %param.6, f32[512,1024]{1,0:T(8,128)} %param.7), kind=kLoop, calls=%fused_computation.9 | loop fusion | flops 2097152 | bytes 6293504 | tf_op jit(solution)/shard_map/convert_element_type | solution.py:17
  11.8 0.0 all-gather.7.cloned.1.call-update
  11.8 0.0 all-gather.11.cloned.1.call-start
  11.9 0.0 copy-done.3
  11.9 1.1 convert_element_type.32
  13.0 0.0 all-gather.11.cloned.1.call-update
  13.0 0.0 all-gather.9.cloned.1.call-start
  13.1 0.5 all-gather.9.cloned.1.call-update
  13.6 0.0 reduce-scatter.2.cloned.1.call-start
  13.7 45.5 %all-gather.5.cloned.1.call-done = bf16[1024,2048]{1,0:T(8,128)(2,1)} async-done(((bf16[128,2048]{1,0:T(8,128)(2,1)}), bf16[1024,2048]{1,0:T(8,128)(2,1)}) %all-gather.5.cloned.1.call-update) | async-done | bytes 4194320 | tf_op jit(solution)/shard_map/all_gather | solution.py:24
  59.2 3.1 multiply_reduce_fusion
  62.3 50.7 %all-gather.7.cloned.1.call-done = bf16[2048,1024]{1,0:T(8,128)(2,1)} async-done(((bf16[512,1024]{1,0:T(8,128)(2,1)}), bf16[2048,1024]{1,0:T(8,128)(2,1)}) %all-gather.7.cloned.1.call-update) | async-done | bytes 4194320 | tf_op jit(solution)/shard_map/all_gather | solution.py:20
  113.0 10.0 %fusion.5 = f32[1024,1024]{1,0:T(8,128)} fusion(bf16[2048,1024]{1,0:T(8,128)(2,1)} %all-gather.7.cloned.1.call-done, bf16[1024,2048]{1,0:T(8,128)(2,1)} %all-gather.5.cloned.1.call-done), kind=kOutput, calls=%fused_computation.14 | convolution fusion | flops 4294967296 | bytes 12582912 | tf_op jit(solution)/shard_map/dot_general | solution.py:10
  123.1 45.0 %all-gather.11.cloned.1.call-done = bf16[2048,1024]{1,0:T(8,128)(2,1)} async-done(((bf16[512,1024]{1,0:T(8,128)(2,1)}), bf16[2048,1024]{1,0:T(8,128)(2,1)}) %all-gather.11.cloned.1.call-update) | async-done | bytes 4194320 | tf_op jit(solution)/shard_map/all_gather | solution.py:22
  168.1 54.9 %all-gather.9.cloned.1.call-done = bf16[2048,1024]{1,0:T(8,128)(2,1)} async-done(((bf16[512,1024]{1,0:T(8,128)(2,1)}), bf16[2048,1024]{1,0:T(8,128)(2,1)}) %all-gather.9.cloned.1.call-update) | async-done | bytes 4194320 | tf_op jit(solution)/shard_map/all_gather | solution.py:21
  222.9 15.9 %convolution_convert_fusion = bf16[1024,2048]{1,0:T(8,128)(2,1)} fusion(bf16[2048,1024]{1,0:T(8,128)(2,1)} %all-gather.11.cloned.1.call-done, f32[1024,1024]{1,0:T(8,128)} %fusion.5, bf16[2048,1024]{1,0:T(8,128)(2,1)} %all-gather.9.cloned.1.call-done, bf16[1024,2048]{1,0:T(8,128)(2,1)} %all-gather.5.cloned.1.call-done, f32[1024]{0:T(1024)S(1)} %add_rsqrt_fusion), kind=kOutput, calls=%fused_computation.8 | convolution fusion | flops 8600420352 | bytes 20975616 | tf_op jit(solution)/shard_map/dot_general | solution.py:25
  238.8 0.0 copy-start.2
  238.8 0.0 reduce-scatter.2.cloned.1.call-update
  238.9 50.1 %reduce-scatter.2.cloned.1.call-done = bf16[128,2048]{1,0:T(8,128)(2,1)} async-done(((bf16[1024,2048]{1,0:T(8,128)(2,1)}), bf16[128,2048]{1,0:T(8,128)(2,1)}) %reduce-scatter.2.cloned.1.call-update) | async-done | bytes 524304 | tf_op jit(solution)/shard_map/reduce_scatter | solution.py:28
  288.9 0.0 copy-done.2
  288.9 2.0 add_convert_fusion
  290.9 0.0 copy-start.1
  290.9 4.8 %copy.12 = bf16[2048,1024]{1,0:T(8,128)(2,1)} copy(bf16[2048,1024]{1,0:T(8,128)(2,1)} %all-gather.7.cloned.1.call-done) | data formatting | bytes 8388608
  295.8 0.0 copy-done.1
  295.8 0.0 copy-start
  295.8 2.1 copy.13
  297.9 1.6 copy-done
  299.5 2.0 copy.14
  (1 shorter events, 0.0 us)
Async XLA Ops:
  7.2 4.7 %copy-start.3 = (f32[512,1024]{1,0:T(8,128)S(1)}, f32[512,1024]{1,0:T(8,128)}, u32[]{:S(2)}) copy-start(f32[512,1024]{1,0:T(8,128)} %param.9) | copy-start | bytes 6291460
  7.2 52.0 %all-gather.5.cloned.1.call-start = ((), (), s32[]{:S(2)}) async-start(), calls=%async_computation.1 | async-start | bytes 4718592 | tf_op jit(solution)/shard_map/all_gather | solution.py:24
  7.9 105.1 %all-gather.7.cloned.1.call-start = ((), (), s32[]{:S(2)}) async-start(), calls=%async_computation.2 | async-start | bytes 5242880 | tf_op jit(solution)/shard_map/all_gather | solution.py:20
  11.8 156.2 %all-gather.11.cloned.1.call-start = ((), (), s32[]{:S(2)}) async-start(), calls=%async_computation.4 | async-start | bytes 5242880 | tf_op jit(solution)/shard_map/all_gather | solution.py:22
  13.0 209.9 %all-gather.9.cloned.1.call-start = ((), (), s32[]{:S(2)}) async-start(), calls=%async_computation.3 | async-start | bytes 5242880 | tf_op jit(solution)/shard_map/all_gather | solution.py:21
  13.6 275.3 %reduce-scatter.2.cloned.1.call-start = ((), (), s32[]{:S(2)}) async-start(), calls=%async_computation.5 | async-start | bytes 4718592 | tf_op jit(solution)/shard_map/reduce_scatter | solution.py:28
  238.8 50.1 %copy-start.2 = (bf16[128,2048]{1,0:T(8,128)(2,1)S(1)}, bf16[128,2048]{1,0:T(8,128)(2,1)}, u32[]{:S(2)}) copy-start(bf16[128,2048]{1,0:T(8,128)(2,1)} %param.5) | copy-start | bytes 1572868
  290.9 4.8 %copy-start.1 = (bf16[2048,1024]{1,0:T(8,128)(2,1)S(1)}, bf16[2048,1024]{1,0:T(8,128)(2,1)}, u32[]{:S(2)}) copy-start(bf16[2048,1024]{1,0:T(8,128)(2,1)} %all-gather.9.cloned.1.call-done) | copy-start | bytes 12582916
  295.8 3.7 %copy-start = (bf16[2048,1024]{1,0:T(8,128)(2,1)S(1)}, bf16[2048,1024]{1,0:T(8,128)(2,1)}, u32[]{:S(2)}) copy-start(bf16[2048,1024]{1,0:T(8,128)(2,1)} %all-gather.11.cloned.1.call-done) | copy-start | bytes 12582916
Sparse Core Ops, SparseCore 0:
  9.6 49.5 all-gather.4
  61.6 51.3 all-gather.6
  115.5 52.5 all-gather.10
  170.3 52.5 all-gather.8
  239.0 49.9 reduce-scatter.1
where the time goes:
time: 308 us
  waiting for transfers between devices  247 us (80%)
  matrix products  25.9 us (8%)
  between operations  13.8 us (4%)
  local copies, waits for them, and re-layouts  10.5 us (3%)
  other arithmetic  10.1 us (3%)
    all_gather x1, waiting for transfers between devices, body(): lax.all_gather(up_local, 'fs', axis=0, tiled=True)  54.9 us
    all_gather x1, waiting for transfers between devices, body(): lax.all_gather(gate_local, 'fs', axis=0, tiled=True)  50.7 us
    reduce_scatter x1, waiting for transfers between devices, body(): lax.psum_scatter(partial_value.astype(jnp.bfloat16), 'tp', scatter_dimens...  50.1 us
    all_gather x1, waiting for transfers between devices, body(): lax.all_gather(tokens, 'tp', axis=0, tiled=True)  45.5 us
    all_gather x1, waiting for transfers between devices, body(): lax.all_gather(down_local, 'fs', axis=0, tiled=True)  45 us
    dot_general x1, matrix products, body(): lax.dot_general(hidden, down_ready, (((1,), (1,)), ((), ())), preferred_e...  15.9 us
    unnamed x11, local copies, waits for them, and re-layouts  10.5 us
    dot_general x1, matrix products, expand_rows(): jnp.dot(rows, gate_ready, preferred_element_type=jnp.float32)  10 us
  transfers between devices with their start and end apart: 5, of which 5 were waited for; matrix products, arithmetic and copies ran while one was open for 6% of the time, Pallas kernels for 0%

commit v1 on v0

v1 whole, which is shorter than its diff:
```python
import functools

import jax
import jax.numpy as jnp
from jax import lax
from jax.experimental import pallas as pl
from jax.experimental.pallas import tpu as pltpu
from jax.sharding import PartitionSpec as P

MESH = pl.DeviceIdType.MESH
GATE, UP, DOWN = 0, 1, 2


def flip(index, bit):
    return index + bit - 2 * bit * ((index // bit) % 2)


def flip_all(index, mask, dims):
    for dim in range(dims):
        if mask >> dim & 1:
            index = flip(index, 1 << dim)
    return index


def span(bits):
    masks = [0]
    for bit in bits:
        masks += [mask | bit for mask in masks]
    return masks


def kernel(
    n_fs, n_z, dims, pieces,
    tok_in, gain, gate_master, up_master, down_master,
    mixed, gate, up, down,
    tok, scale, gate_acc, up_acc, hidden, pair_own, pair_send, pair_recv, z_send, z_recv,
    w_sent, w_got, t_sent, t_got, s_sent, s_got, p_sent, p_got, z_sent, z_got,
):
    fs, tp = lax.axis_index("fs"), lax.axis_index("tp")
    z, core = tp // 2, tp % 2
    sibling = z * 2 + 1 - core
    rows, cols = gate_master.shape
    part = rows // dims
    own_tok = tok_in.shape[0]
    half = n_z * own_tok
    total = 2 * half
    width = rows // pieces
    masters, ready = (gate_master, up_master, down_master), (gate, up, down)

    def z_peer(k):
        return ((z + k) % n_z) * 2 + core

    barrier = pltpu.get_barrier_semaphore()
    for dim in range(dims):
        pl.semaphore_signal(barrier, 1, device_id={"fs": flip(fs, 1 << dim)}, device_id_type=MESH)
    for k in range(1, n_z):
        pl.semaphore_signal(barrier, 1, device_id={"tp": z_peer(k)}, device_id_type=MESH)
    pl.semaphore_signal(barrier, 1, device_id={"tp": sibling}, device_id_type=MESH)
    pl.semaphore_wait(barrier, dims + n_z)

    def block(w, mask, p, count=1):
        start = flip_all(fs, mask, dims) * rows + p * part
        return ready[w].at[pl.ds(pl.multiple_of(start, part), part * count), :]

    def order(p):
        return [1 << ((p + s) % dims) for s in range(dims)]

    def weight_copy(w, p, stage, held):
        bit = order(p)[stage]
        mask = held | bit
        return pltpu.make_async_remote_copy(
            src_ref=block(w, held, p), dst_ref=block(w, held, p),
            send_sem=w_sent.at[w, p, mask], recv_sem=w_got.at[w, p, mask],
            device_id={"fs": flip(fs, bit)}, device_id_type=MESH,
        )

    arrivals = {}
    started, arrived = [], set()
    for p in range(dims):
        for stage in range(dims):
            for held in span(order(p)[:stage]):
                arrivals[p, held | order(p)[stage]] = (stage, held)

    def send(w, p, stage, held):
        copy = weight_copy(w, p, stage, held)
        copy.start()
        started.append(copy)

    def need(w, p, mask):
        if mask and (w, p, mask) not in arrived:
            arrived.add((w, p, mask))
            stage, held = arrivals[p, mask]
            pltpu.make_async_remote_copy(
                src_ref=block(w, mask, p), dst_ref=block(w, mask, p),
                send_sem=w_sent.at[w, p, mask], recv_sem=w_got.at[w, p, mask],
                device_id={"fs": flip(fs, order(p)[stage])}, device_id_type=MESH,
            ).wait_recv()

    def relays(ws):
        for stage in range(1, dims):
            for w in ws:
                for p in range(dims):
                    for mask in span(order(p)[:stage]):
                        if mask:
                            need(w, p, mask)
                            send(w, p, stage, mask)

    def prepare(w, p):
        mine = slice(p * part, (p + 1) * part)
        value = masters[w][mine, :]
        if w != DOWN:
            value = gain[mine, :] * value
        block(w, 0, p)[...] = value.astype(jnp.bfloat16)

    for w in (GATE, UP):
        for p in range(dims):
            prepare(w, p)
            send(w, p, 0, 0)

    def tok_rows(c, chip):
        start = (c * n_z + chip) * own_tok
        return tok.at[pl.ds(pl.multiple_of(start, own_tok), own_tok), :]

    def tok_z(k):
        return pltpu.make_async_remote_copy(
            src_ref=tok_in, dst_ref=tok_rows(core, z), send_sem=t_sent.at[k], recv_sem=t_got.at[k],
            device_id={"tp": z_peer(k)}, device_id_type=MESH,
        )

    def tok_sibling(k, src, slot):
        return pltpu.make_async_remote_copy(
            src_ref=src, dst_ref=slot, send_sem=s_sent.at[k], recv_sem=s_got.at[k],
            device_id={"tp": sibling}, device_id_type=MESH,
        )

    for k in range(1, n_z):
        copy = tok_z(k)
        copy.start()
        started.append(copy)
    copy = tok_sibling(0, tok_in, tok_rows(core, z))
    copy.start()
    started.append(copy)
    for w in (GATE, UP):
        for p in range(dims):
            for stage in range(1, dims):
                send(w, p, stage, 0)
    tok_rows(core, z)[...] = tok_in[...]
    for p in range(dims):
        prepare(DOWN, p)

    relays((GATE, UP))
    for p in range(dims):
        send(DOWN, p, 0, 0)
    for p in range(dims):
        for stage in range(1, dims):
            send(DOWN, p, stage, 0)

    for k in range(1, n_z):
        slot = tok_rows(core, (z + n_z - k) % n_z)
        pltpu.make_async_remote_copy(
            src_ref=slot, dst_ref=slot, send_sem=t_sent.at[k], recv_sem=t_got.at[k],
            device_id={"tp": z_peer(k)}, device_id_type=MESH,
        ).wait_recv()
        copy = tok_sibling(k, slot, slot)
        copy.start()
        started.append(copy)
    for k in range(n_z):
        slot = tok_rows(1 - core, (z + n_z - k) % n_z)
        tok_sibling(k, slot, slot).wait_recv()

    tile_m, tile_n = min(256, total), min(512, cols)
    tile_s = min(64, total)

    @pl.loop(0, total // tile_s)
    def _(i):
        at = pl.ds(pl.multiple_of(i * tile_s, tile_s), tile_s)
        wide = tok[at, :].astype(jnp.float32)
        scale[at, :] = lax.rsqrt(jnp.mean(wide * wide, axis=1, keepdims=True) + 1e-06)

    for mask in range(n_fs):
        for w in (GATE, UP):
            for p in range(dims):
                need(w, p, mask)
        owner = flip_all(fs, mask, dims)
        deep = pl.ds(pl.multiple_of(owner * rows, rows), rows)
        first, last = mask == 0, mask == n_fs - 1

        @pl.loop(0, (total // tile_m) * (cols // tile_n))
        def _(i):
            across = cols // tile_n
            at = pl.ds(pl.multiple_of((i // across) * tile_m, tile_m), tile_m)
            to = pl.ds(pl.multiple_of((i % across) * tile_n, tile_n), tile_n)
            x = tok[at, deep]
            g = jnp.dot(x, gate[deep, to], preferred_element_type=jnp.float32)
            u = jnp.dot(x, up[deep, to], preferred_element_type=jnp.float32)
            if not first:
                g = g + gate_acc[at, to]
                u = u + up_acc[at, to]
            if last:
                g = scale[at, :] * g
                u = scale[at, :] * u
                hidden[at, to] = (g / (1.0 + jnp.exp(-g)) * u).astype(jnp.bfloat16)
            else:
                gate_acc[at, to] = g
                up_acc[at, to] = u

    def product(parity, start, out, add=None):
        tile = min(256, half)

        @pl.loop(0, half // tile)
        def _(i):
            at = pl.ds(pl.multiple_of(i * tile, tile), tile)
            src = pl.ds(pl.multiple_of(parity * half + i * tile, tile), tile)
            value = lax.dot_general(
                hidden[src, :], down[pl.ds(pl.multiple_of(start, width), width), :],
                (((1,), (1,)), ((), ())), preferred_element_type=jnp.float32,
            )
            out[at, :] = value.astype(out.dtype)

    def pair_copy(n):
        return pltpu.make_async_remote_copy(
            src_ref=pair_send.at[n], dst_ref=pair_recv.at[n],
            send_sem=p_sent.at[n], recv_sem=p_got.at[n],
            device_id={"tp": sibling}, device_id_type=MESH,
        )

    def z_copy(n, k):
        slot = pl.ds(pl.multiple_of(((z + k) % n_z) * own_tok, own_tok), own_tok)
        return pltpu.make_async_remote_copy(
            src_ref=z_send.at[n, slot, :], dst_ref=z_recv.at[n, k - 1],
            send_sem=z_sent.at[n, k], recv_sem=z_got.at[n, k],
            device_id={"tp": z_peer(k)}, device_id_type=MESH,
        )

    chunks = []
    late = sorted(
        ((mask, q) for mask in range(n_fs) for q in range(pieces)),
        key=lambda c: (
            0 if c[0] == 0 else 1 + max(
                2 * arrivals[p, c[0]][0] + bin(c[0]).count("1") * 4
                for p in ((c[1],) if pieces == dims else range(dims))
            ), c[0], c[1],
        ),
    )

    def finish(n):
        pair_copy(n).wait_recv()
        z_send[n] = (pair_own[n % 2] + pair_recv[n].astype(jnp.float32)).astype(jnp.bfloat16)
        for k in range(n_z - 1, 0, -1):
            copy = z_copy(n, k)
            copy.start()
            started.append(copy)

    relayed = False
    for n, (mask, q) in enumerate(late):
        if mask and not relayed:
            relayed = True
            relays((DOWN,))
        for p in (q,) if pieces == dims else range(dims):
            need(DOWN, p, mask)
        start = flip_all(fs, mask, dims) * rows + q * width
        product(1 - core, start, pair_send.at[n])
        copy = pair_copy(n)
        copy.start()
        started.append(copy)
        product(core, start, pair_own.at[n % 2])
        chunks.append(start)
        finish(n)

    for n, start in enumerate(chunks):
        for k in range(1, n_z):
            z_copy(n, k).wait_recv()
        mine = pl.ds(pl.multiple_of(z * own_tok, own_tok), own_tok)
        branch = z_send[n, mine, :].astype(jnp.float32)
        for k in range(1, n_z):
            branch = branch + z_recv[n, k - 1].astype(jnp.float32)
        to = pl.ds(pl.multiple_of(start, width), width)
        mixed[:, to] = (tok_in[:, to].astype(jnp.float32) + 0.5 * branch).astype(jnp.bfloat16)

    for copy in started:
        copy.wait_send()


def body(n_fs, n_tp, tokens, norm_gain, gate_master, up_master, down_master):
    own_tok, depth = tokens.shape
    rows, cols = gate_master.shape
    dims = n_fs.bit_length() - 1
    n_z = n_tp // 2
    half, total = n_z * own_tok, n_tp * own_tok
    part = rows // dims
    pieces = dims if part % 128 == 0 else 1
    width, count = rows // pieces, n_fs * pieces
    bf16, f32 = jnp.bfloat16, jnp.float32
    dma = pltpu.SemaphoreType.DMA
    vmem = pl.BlockSpec(memory_space=pltpu.VMEM)
    return pl.pallas_call(
        functools.partial(kernel, n_fs, n_z, dims, pieces),
        out_shape=(jax.ShapeDtypeStruct((own_tok, depth), bf16),)
        + tuple(pltpu.VMEM((n_fs * rows, cols), bf16) for _ in range(3)),
        in_specs=[vmem] * 5,
        out_specs=(vmem,) * 4,
        scratch_shapes=[
            pltpu.VMEM((total, depth), bf16),
            pltpu.VMEM((total, 1), f32),
            pltpu.VMEM((total, cols), f32),
            pltpu.VMEM((total, cols), f32),
            pltpu.VMEM((total, cols), bf16),
            pltpu.VMEM((2, half, width), f32),
            pltpu.VMEM((count, half, width), bf16),
            pltpu.VMEM((count, half, width), bf16),
            pltpu.VMEM((count, half, width), bf16),
            pltpu.VMEM((count, n_z - 1, own_tok, width), bf16),
            dma((3, dims, n_fs)), dma((3, dims, n_fs)),
            dma((n_z,)), dma((n_z,)),
            dma((n_z,)), dma((n_z,)),
            dma((count,)), dma((count,)),
            dma((count, n_z)), dma((count, n_z)),
        ],
        compiler_params=pltpu.CompilerParams(
            collective_id=0, has_side_effects=True, vmem_limit_bytes=40 * 1024 * 1024
        ),
    )(tokens, norm_gain[:, None], gate_master, up_master, down_master)


def solution(mesh):
    in_specs = (P(("fs", "tp"), None), P("fs"), P("fs", "tp"), P("fs", "tp"), P("fs", "tp"))
    out_specs = (P(("fs", "tp"), None), P(None, "tp"), P(None, "tp"), P(None, "tp"))
    step = functools.partial(body, mesh.shape["fs"], mesh.shape["tp"])
    return jax.shard_map(step, mesh=mesh, in_specs=in_specs, out_specs=out_specs, check_vma=False)
```

time: 308 us -> 142 us (0.46)
  waiting for transfers between devices: 247 us -> 0 us
  Pallas kernels: 0 us -> 132 us
  matrix products: 25.9 us -> 0 us
  between operations: 13.8 us -> 0.66 us
  other arithmetic: 10.1 us -> 0 us
    all_gather x4 -> x0, waiting for transfers between devices: 196 us -> none  [the longest x1 54.9 us: body(): lax.all_gather(up_local, 'fs', axis=0, tiled=True)]
    pallas_call x0 -> x1, Pallas kernels: none -> 132 us  [body(): pl.pallas_call(functools.partial(kernel, n_fs, n_z, dims, pieces), out_sh...]
    reduce_scatter x1 -> x0, waiting for transfers between devices: 50.1 us -> none  [body(): lax.psum_scatter(partial_value.astype(jnp.bfloat16), 'tp', scatter_dimens...]
    dot_general x2 -> x0, matrix products: 25.9 us -> none  [the longest x1 15.9 us: body(): lax.dot_general(hidden, down_ready, (((1,), (1,)), ((), ())), preferred_e...]
    convert_element_type x3 -> x0, other arithmetic: 6.97 us -> none  [the longest x1 3.85 us: body(): up_local = (norm_gain[:, None] * up_master).astype(jnp.bfloat16)]
    unnamed x11 -> x6, local copies, waits for them, and re-layouts: 10.5 us -> 7.87 us
  transfers between devices with their start and end apart: 5 -> 0, of which waited for: 5 -> 0; matrix products, arithmetic and copies ran while one was open for 6% -> 0% of each run, Pallas kernels for 0% -> 0%
where the time goes in v1:
time: 142 us; the launch traced here: 141 us
  Pallas kernels  132 us (93%)
  local copies, waits for them, and re-layouts  8.69 us (6%)
    pallas_call x1, Pallas kernels, body(): pl.pallas_call(functools.partial(kernel, n_fs, n_z, dims, pieces), out_sh...  132 us
    unnamed x6, local copies, waits for them, and re-layouts  7.87 us

profile of v1, /device:TPU:0, one launch (start us, length us, event | category | flops | bytes accessed | tf_op | source)
XLA Modules:
  0.0 141.4 jit_solution(12289485308041450792)
XLA Ops:
  0.6 0.8 copy.9.gain
  1.5 0.0 copy-start
  1.5 1.0 copy-done
  2.5 132.1 %shard_map.84 = (bf16[128,2048]{1,0:T(8,128)(2,1)S(1)}, bf16[2048,1024]{1,0:T(8,128)(2,1)S(1)}, bf16[2048,1024]{1,0:T(8,128)(2,1)S(1)}, bf16[2048,1024]{1,0:T(8,128)(2,1)S(1)}) custom-call(bf16[128,2048]{1,0:T(8,128)(2,1)S(1)} %copy-done, f32[512,1]{1,0:T(8,128)S(1)} %copy.9.gain, f32[512,1024]{1,0:T(8,128)} %gate_master.1, f32[512,1024]{1,0:T(8,128)} %up_master.1, ...), custom_call_target="tpu_custom_call" | custom-call | tf_op jit(solution)/shard_map/pallas_call | solution.py:296
  134.6 2.0 %copy.14 = bf16[2048,1024]{1,0:T(8,128)(2,1)} copy(bf16[2048,1024]{1,0:T(8,128)(2,1)S(1)} %get-tuple-element.5) | data formatting | bytes 8388608
  136.6 2.0 %copy.15 = bf16[2048,1024]{1,0:T(8,128)(2,1)} copy(bf16[2048,1024]{1,0:T(8,128)(2,1)S(1)} %get-tuple-element.6) | data formatting | bytes 8388608
  138.6 2.0 %copy.16 = bf16[2048,1024]{1,0:T(8,128)(2,1)} copy(bf16[2048,1024]{1,0:T(8,128)(2,1)S(1)} %get-tuple-element.7) | data formatting | bytes 8388608
  140.6 0.8 copy.17
Async XLA Ops:
  1.5 1.0 copy-start

commit v2 on v1

v2 whole, which is shorter than its diff:
```python
import functools

import jax
import jax.numpy as jnp
from jax import lax
from jax.experimental import pallas as pl
from jax.experimental.pallas import tpu as pltpu
from jax.sharding import PartitionSpec as P

MESH = pl.DeviceIdType.MESH
GATE, UP, DOWN = 0, 1, 2


def flip(index, bit):
    return index + bit - 2 * bit * ((index // bit) % 2)


def flip_all(index, mask, dims):
    for dim in range(dims):
        if mask >> dim & 1:
            index = flip(index, 1 << dim)
    return index


def span(bits):
    masks = [0]
    for bit in bits:
        masks += [mask | bit for mask in masks]
    return masks


def kernel(
    n_fs, n_z, dims, halves, pieces,
    tok_hbm, gain_hbm, gate_hbm, up_hbm, down_hbm,
    mixed, gate, up, down,
    tok_in, gain_row, gain, masters, tok, scale, gate_acc, up_acc, hidden, pair_own, pair_send, pair_recv, z_send, z_recv, ahead,
    w_sent, w_got, t_sent, t_got, s_sent, s_got, p_sent, p_got, z_sent, z_got, a_sent, a_got, loaded,
):
    fs, tp = lax.axis_index("fs"), lax.axis_index("tp")
    z, core = tp // 2, tp % 2
    sibling = z * 2 + 1 - core
    rows, cols = gate_hbm.shape
    part = rows // dims
    own_tok = tok_in.shape[0]
    half = n_z * own_tok
    total = 2 * half
    width = rows // pieces
    ready = (gate, up, down)

    loads = {}
    reads = [("gain", gain_hbm, gain_row)]
    for p in range(dims):
        mine = pl.ds(p * part, part)
        reads.append(((GATE, p), gate_hbm.at[mine, :], masters.at[GATE, mine, :]))
    for p in range(dims):
        mine = pl.ds(p * part, part)
        reads.append(((UP, p), up_hbm.at[mine, :], masters.at[UP, mine, :]))
    reads.append(("tok", tok_hbm, tok_in))
    reads.append(((DOWN, 0), down_hbm, masters.at[DOWN]))
    for n, (name, src, dst) in enumerate(reads):
        loads[name] = pltpu.make_async_copy(src, dst, loaded.at[n])
        loads[name].start()

    def z_peer(k):
        return ((z + k) % n_z) * 2 + core

    barrier = pltpu.get_barrier_semaphore()
    for dim in range(dims):
        pl.semaphore_signal(barrier, 1, device_id={"fs": flip(fs, 1 << dim)}, device_id_type=MESH)
    for k in range(1, n_z):
        pl.semaphore_signal(barrier, 1, device_id={"tp": z_peer(k)}, device_id_type=MESH)
    pl.semaphore_signal(barrier, 1, device_id={"tp": sibling}, device_id_type=MESH)
    pl.semaphore_wait(barrier, dims + n_z)

    loads["gain"].wait()
    for n in range(rows // 128):
        line = gain_row[:, n * 128:(n + 1) * 128]
        gain[n * 128:(n + 1) * 128, :] = jnp.transpose(jnp.broadcast_to(line, (128, 128)))

    cuts = (1, 1, halves)

    def block(w, mask, p, h):
        tall = part // cuts[w]
        start = flip_all(fs, mask, dims) * rows + p * part + h * tall
        return ready[w].at[pl.ds(pl.multiple_of(start, tall), tall), :]

    def order(p):
        return [1 << ((p + s) % dims) for s in range(dims)]

    arrivals = {
        (p, held | order(p)[stage]): stage
        for p in range(dims) for stage in range(dims) for held in span(order(p)[:stage])
    }
    started, arrived = [], set()

    def weight_copy(w, p, h, held, mask, stage):
        return pltpu.make_async_remote_copy(
            src_ref=block(w, held, p, h), dst_ref=block(w, held, p, h),
            send_sem=w_sent.at[w, p, h, mask], recv_sem=w_got.at[w, p, h, mask],
            device_id={"fs": flip(fs, order(p)[stage])}, device_id_type=MESH,
        )

    def launch(copy):
        copy.start()
        started.append(copy)

    def send(w, p, h, stage, held):
        launch(weight_copy(w, p, h, held, held | order(p)[stage], stage))

    def need(w, p, h, mask):
        if mask and (w, p, h, mask) not in arrived:
            arrived.add((w, p, h, mask))
            stage = arrivals[p, mask]
            weight_copy(w, p, h, mask, mask, stage).wait_recv()
            for later in range(stage + 1, dims):
                send(w, p, h, later, mask)

    def relays(ws):
        for stage in range(dims - 1):
            for w in ws:
                for p in range(dims):
                    for held in span(order(p)[:stage]):
                        for h in range(cuts[w]):
                            need(w, p, h, held | order(p)[stage])

    def prepare(w, p):
        mine = slice(p * part, (p + 1) * part)
        if (w, p) in loads:
            loads[w, p].wait()
        value = masters[w, mine, :]
        if w != DOWN:
            value = gain[mine, 0:1] * value
        ready[w][pl.ds(pl.multiple_of(fs * rows + p * part, part), part), :] = value.astype(jnp.bfloat16)

    for p in range(dims):
        prepare(GATE, p)
        send(GATE, p, 0, 0, 0)
    for p in range(dims):
        prepare(UP, p)
        send(UP, p, 0, 0, 0)

    def tok_rows(c, chip):
        start = (c * n_z + chip) * own_tok
        return tok.at[pl.ds(pl.multiple_of(start, own_tok), own_tok), :]

    def tok_z(k):
        return pltpu.make_async_remote_copy(
            src_ref=tok_in, dst_ref=tok_rows(core, z), send_sem=t_sent.at[k], recv_sem=t_got.at[k],
            device_id={"tp": z_peer(k)}, device_id_type=MESH,
        )

    def tok_sibling(k, src, slot):
        return pltpu.make_async_remote_copy(
            src_ref=src, dst_ref=slot, send_sem=s_sent.at[k], recv_sem=s_got.at[k],
            device_id={"tp": sibling}, device_id_type=MESH,
        )

    loads["tok"].wait()
    for k in range(1, n_z):
        launch(tok_z(k))
    launch(tok_sibling(0, tok_in, tok_rows(core, z)))
    for w in (GATE, UP):
        for p in range(dims):
            for stage in range(1, dims):
                send(w, p, 0, stage, 0)
    tok_rows(core, z)[...] = tok_in[...]
    for p in range(dims):
        prepare(DOWN, p)

    relays((GATE, UP))
    for stage in range(dims):
        for h in range(halves):
            for p in range(dims):
                send(DOWN, p, h, stage, 0)

    for k in range(1, n_z):
        slot = tok_rows(core, (z + n_z - k) % n_z)
        pltpu.make_async_remote_copy(
            src_ref=slot, dst_ref=slot, send_sem=t_sent.at[k], recv_sem=t_got.at[k],
            device_id={"tp": z_peer(k)}, device_id_type=MESH,
        ).wait_recv()
        launch(tok_sibling(k, slot, slot))
    for k in range(n_z):
        slot = tok_rows(1 - core, (z + n_z - k) % n_z)
        tok_sibling(k, slot, slot).wait_recv()

    tile_m, tile_n = min(256, total), min(512, cols)
    tile_s = min(64, total)

    @pl.loop(0, total // tile_s)
    def _(i):
        at = pl.ds(pl.multiple_of(i * tile_s, tile_s), tile_s)
        wide = tok[at, :].astype(jnp.float32)
        scale[at, :] = lax.rsqrt(jnp.mean(wide * wide, axis=1, keepdims=True) + 1e-06)

    for mask in range(n_fs):
        for w in (GATE, UP):
            for p in range(dims):
                need(w, p, 0, mask)
        owner = flip_all(fs, mask, dims)
        deep = pl.ds(pl.multiple_of(owner * rows, rows), rows)
        first, last = mask == 0, mask == n_fs - 1

        @pl.loop(0, (total // tile_m) * (cols // tile_n))
        def _(i):
            across = cols // tile_n
            at = pl.ds(pl.multiple_of((i // across) * tile_m, tile_m), tile_m)
            to = pl.ds(pl.multiple_of((i % across) * tile_n, tile_n), tile_n)
            x = tok[at, deep]
            g = jnp.dot(x, gate[deep, to], preferred_element_type=jnp.float32)
            u = jnp.dot(x, up[deep, to], preferred_element_type=jnp.float32)
            if not first:
                g = g + gate_acc[at, to]
                u = u + up_acc[at, to]
            if last:
                g = scale[at, :] * g
                u = scale[at, :] * u
                hidden[at, to] = (g / (1.0 + jnp.exp(-g)) * u).astype(jnp.bfloat16)
            else:
                gate_acc[at, to] = g
                up_acc[at, to] = u

    def product(parity, start, out, add=None):
        tile = min(256, half)

        @pl.loop(0, half // tile)
        def _(i):
            at = pl.ds(pl.multiple_of(i * tile, tile), tile)
            src = pl.ds(pl.multiple_of(parity * half + i * tile, tile), tile)
            value = lax.dot_general(
                hidden[src, :], down[pl.ds(pl.multiple_of(start, width), width), :],
                (((1,), (1,)), ((), ())), preferred_element_type=jnp.float32,
            )
            out[at, :] = value.astype(out.dtype)

    def pair_copy(n):
        return pltpu.make_async_remote_copy(
            src_ref=pair_send.at[n], dst_ref=pair_recv.at[n],
            send_sem=p_sent.at[n], recv_sem=p_got.at[n],
            device_id={"tp": sibling}, device_id_type=MESH,
        )

    def z_copy(n, k):
        slot = pl.ds(pl.multiple_of(((z + k) % n_z) * own_tok, own_tok), own_tok)
        return pltpu.make_async_remote_copy(
            src_ref=z_send.at[n, slot, :], dst_ref=z_recv.at[n, k - 1],
            send_sem=z_sent.at[n, k], recv_sem=z_got.at[n, k],
            device_id={"tp": z_peer(k)}, device_id_type=MESH,
        )

    merge = n_z > 2

    def goes_ahead(k):
        return ((z == 0) & (k == n_z - 1)) | ((z == n_z - 1) & (k == 1))

    def ahead_copy(n, k):
        slot = pl.ds(pl.multiple_of(((z + k) % n_z) * own_tok, own_tok), own_tok)
        return pltpu.make_async_remote_copy(
            src_ref=z_send.at[n, slot, :], dst_ref=ahead.at[n], send_sem=a_sent.at[n], recv_sem=a_got.at[n],
            device_id={"tp": (z + 1 if k == n_z - 1 else z - 1) * 2 + core}, device_id_type=MESH,
        )

    def joins(k):
        return ((z == 1) & (k == n_z - 2)) | ((z == n_z - 2) & (k == 2))

    def finish(n):
        pair_copy(n).wait_recv()
        z_send[n] = (pair_own[n % 2] + pair_recv[n].astype(jnp.float32)).astype(jnp.bfloat16)
        if merge:
            for k in (1, n_z - 1):
                @pl.when(goes_ahead(k))
                def _():
                    ahead_copy(n, k).start()
        for k in range(n_z - 1, 0, -1):
            if merge:
                @pl.when(jnp.logical_not(goes_ahead(k) | joins(k)))
                def _():
                    z_copy(n, k).start()
            else:
                z_copy(n, k).start()

    def join(n):
        if merge:
            for k in sorted({2, n_z - 2}):
                @pl.when(joins(k))
                def _():
                    slot = pl.ds(pl.multiple_of(((z + k) % n_z) * own_tok, own_tok), own_tok)
                    pltpu.make_async_remote_copy(
                        src_ref=ahead.at[n], dst_ref=ahead.at[n], send_sem=a_sent.at[n], recv_sem=a_got.at[n],
                        device_id={"tp": sibling}, device_id_type=MESH,
                    ).wait_recv()
                    both = z_send[n, slot, :].astype(jnp.float32) + ahead[n].astype(jnp.float32)
                    z_send[n, slot, :] = both.astype(jnp.bfloat16)
                    z_copy(n, k).start()

    def when_block(mask, p, h):
        return (0,) if mask == 0 else (1, bin(mask).count("1") > 1, arrivals[p, mask], h, p)

    blocks = [(mask, p, h) for mask in range(n_fs) for p in range(dims) for h in range(halves)]
    if pieces == 1:
        chunks = [[(mask, p, h) for p in range(dims) for h in range(halves)] for mask in range(n_fs)]
    else:
        chunks = [[b] for b in sorted(blocks, key=lambda b: when_block(*b))]
    starts = []
    for n, chunk in enumerate(chunks):
        for mask, p, h in chunk:
            need(DOWN, p, h, mask)
        mask, p, h = chunk[0]
        start = flip_all(fs, mask, dims) * rows + p * part + h * width
        starts.append(start)
        product(1 - core, start, pair_send.at[n])
        launch(pair_copy(n))
        if n:
            finish(n - 1)
        if n > 1:
            join(n - 2)
        product(core, start, pair_own.at[n % 2])
    finish(len(chunks) - 1)
    for n in range(max(0, len(chunks) - 2), len(chunks)):
        join(n)

    for n, start in enumerate(starts):
        mine = pl.ds(pl.multiple_of(z * own_tok, own_tok), own_tok)
        to = pl.ds(pl.multiple_of(start, width), width)
        branch = z_send[n, mine, :].astype(jnp.float32)
        for k in range(1, n_z):
            if merge and k in (1, n_z - 1):
                far = ((z == n_z - 1) & (k == n_z - 1)) | ((z == 0) & (k == 1))

                @pl.when(jnp.logical_not(far))
                def _():
                    z_copy(n, k).wait_recv()

                @pl.when(far)
                def _():
                    z_recv[n, k - 1] = jnp.zeros((own_tok, width), jnp.bfloat16)
            else:
                z_copy(n, k).wait_recv()
            branch = branch + z_recv[n, k - 1].astype(jnp.float32)
        mixed[:, to] = (tok_in[:, to].astype(jnp.float32) + 0.5 * branch).astype(jnp.bfloat16)

    for n in range(len(chunks)):
        for k in range(1, n_z):
            if merge and k in (1, n_z - 1):
                @pl.when(goes_ahead(k))
                def _():
                    ahead_copy(n, k).wait_send()

                @pl.when(jnp.logical_not(goes_ahead(k)))
                def _():
                    z_copy(n, k).wait_send()
            else:
                z_copy(n, k).wait_send()
    for copy in started:
        copy.wait_send()


def store(*refs):
    count = len(refs) // 2
    done = refs[-1]
    copies = []
    for n in range(count):
        tall = refs[n].shape[0] // 2
        for h in range(2):
            at = pl.ds(h * tall, tall)
            copies.append(pltpu.make_async_copy(refs[n].at[at, :], refs[count + n].at[at, :], done.at[n, h]))
            copies[-1].start()
    for copy in copies:
        copy.wait()


def body(n_fs, n_tp, tokens, norm_gain, gate_master, up_master, down_master):
    own_tok, depth = tokens.shape
    rows, cols = gate_master.shape
    dims = n_fs.bit_length() - 1
    n_z = n_tp // 2
    half, total = n_z * own_tok, n_tp * own_tok
    part = rows // dims
    halves = part // 128 if part % 128 == 0 else 1
    pieces = dims * halves if part % 128 == 0 else 1
    width, count = rows // pieces, n_fs * pieces
    bf16, f32 = jnp.bfloat16, jnp.float32
    dma = pltpu.SemaphoreType.DMA
    vmem = pl.BlockSpec(memory_space=pltpu.VMEM)
    hbm = pl.BlockSpec(memory_space=pltpu.HBM)
    operands = (tokens, norm_gain[None, :], gate_master, up_master, down_master)
    results = pl.pallas_call(
        functools.partial(kernel, n_fs, n_z, dims, halves, pieces),
        out_shape=(pltpu.VMEM((own_tok, depth), bf16),)
        + tuple(pltpu.VMEM((n_fs * rows, cols), bf16) for _ in range(3)),
        in_specs=[hbm] * 5,
        out_specs=(vmem,) * 4,
        scratch_shapes=[
            pltpu.VMEM((own_tok, depth), bf16),
            pltpu.VMEM((1, rows), f32),
            pltpu.VMEM((rows, 128), f32),
            pltpu.VMEM((3, rows, cols), f32),
            pltpu.VMEM((total, depth), bf16),
            pltpu.VMEM((total, 1), f32),
            pltpu.VMEM((total, cols), f32),
            pltpu.VMEM((total, cols), f32),
            pltpu.VMEM((total, cols), bf16),
            pltpu.VMEM((2, half, width), f32),
            pltpu.VMEM((count, half, width), bf16),
            pltpu.VMEM((count, half, width), bf16),
            pltpu.VMEM((count, half, width), bf16),
            pltpu.VMEM((count, n_z - 1, own_tok, width), bf16),
            pltpu.VMEM((count, own_tok, width), bf16),
            dma((3, dims, halves, n_fs)), dma((3, dims, halves, n_fs)),
            dma((n_z,)), dma((n_z,)),
            dma((n_z,)), dma((n_z,)),
            dma((count,)), dma((count,)),
            dma((count, n_z)), dma((count, n_z)),
            dma((count,)), dma((count,)),
            dma((2 * dims + 3,)),
        ],
        compiler_params=pltpu.CompilerParams(
            collective_id=0, has_side_effects=True, vmem_limit_bytes=40 * 1024 * 1024
        ),
    )(*(pltpu.with_memory_space_constraint(value, pltpu.HBM) for value in operands))
    return pl.pallas_call(
        store,
        out_shape=tuple(jax.ShapeDtypeStruct(result.shape, result.dtype) for result in results),
        in_specs=[vmem] * 4,
        out_specs=(hbm,) * 4,
        scratch_shapes=[dma((4, 2))],
        compiler_params=pltpu.CompilerParams(vmem_limit_bytes=1024 * 1024),
    )(*(pltpu.with_memory_space_constraint(result, pltpu.VMEM) for result in results))


def solution(mesh):
    in_specs = (P(("fs", "tp"), None), P("fs"), P("fs", "tp"), P("fs", "tp"), P("fs", "tp"))
    out_specs = (P(("fs", "tp"), None), P(None, "tp"), P(None, "tp"), P(None, "tp"))
    step = functools.partial(body, mesh.shape["fs"], mesh.shape["tp"])
    return jax.shard_map(step, mesh=mesh, in_specs=in_specs, out_specs=out_specs, check_vma=False)
```

time: 142 us -> 128 us (0.901)
  local copies, waits for them, and re-layouts: 8.69 us -> 0 us
  Pallas kernels: 132 us -> 127 us
    unnamed x6 -> x0, local copies, waits for them, and re-layouts: 7.87 us -> none
    pallas_call x1 -> x2, Pallas kernels: 132 us -> 127 us  [the longest x1 122 us: body(): pl.pallas_call(functools.partial(kernel, n_fs, n_z, dims, halves, pieces)...]
where the time goes in v2:
time: 128 us
  Pallas kernels  127 us (99%)
    pallas_call x1, Pallas kernels, body(): pl.pallas_call(functools.partial(kernel, n_fs, n_z, dims, halves, pieces)...  122 us
    pallas_call x1, Pallas kernels, body(): pl.pallas_call(store, out_shape=tuple((jax.ShapeDtypeStruct(result.shape,...  4.84 us

profile of v2, /device:TPU:0, one launch (start us, length us, event | category | flops | bytes accessed | tf_op | source)
XLA Modules:
  0.0 127.7 jit_solution(9190816744762410155)
XLA Ops:
  0.6 122.2 %shard_map.84 = (bf16[128,2048]{1,0:T(8,128)(2,1)S(1)}, bf16[2048,1024]{1,0:T(8,128)(2,1)S(1)}, bf16[2048,1024]{1,0:T(8,128)(2,1)S(1)}, bf16[2048,1024]{1,0:T(8,128)(2,1)S(1)}) custom-call(bf16[128,2048]{1,0:T(8,128)(2,1)} %tok_hbm.1, f32[1,512]{1,0:T(1,128)} %bitcast.1, f32[512,1024]{1,0:T(8,128)} %gate_hbm.1, f32[512,1024]{1,0:T(8,128)} %up_hbm.1, ...), custom_call_target="tpu_custom_call" | custom-call | tf_op jit(solution)/shard_map/pallas_call | solution.py:387
  122.9 4.8 %shard_map.85 = (bf16[128,2048]{1,0:T(8,128)(2,1)}, bf16[2048,1024]{1,0:T(8,128)(2,1)}, bf16[2048,1024]{1,0:T(8,128)(2,1)}, bf16[2048,1024]{1,0:T(8,128)(2,1)}) custom-call(bf16[128,2048]{1,0:T(8,128)(2,1)S(1)} %get-tuple-element.8.refs_0_, bf16[2048,1024]{1,0:T(8,128)(2,1)S(1)} %get-tuple-element.9.refs_1_, ...), custom_call_target="tpu_custom_call" | custom-call | tf_op jit(solution)/shard_map/pallas_call | solution.py:421
